TPU v7x, 32 devices: a whole 2x2x4 slice. The times are simulated.
32 devices in a mesh: ep: 8 (over z, x), tp: 4 (over y, core).
Axes of the slice: x: 2, y: 2, z: 4, core: 2. Of those that a mesh axis runs over, the one named last changes fastest.
Arguments:
- tokens: bfloat16 [1024, 2048], P('ep'), may hold values from -6 to 6
- routing: int32 [1024, 2], P('ep'), may hold values from 0 to 7, all different within a row; in each aligned block of 128 rows (0 to 127, 128 to 255, ...) at most 56 rows name the same one
- router_weight: bfloat16 [2048, 8], replicated, may hold values from -0.125 to 0.125
- gate_weight: bfloat16 [8, 2048, 2048], P('ep', None, 'tp'), may hold values from -0.125 to 0.125
- up_weight: bfloat16 [8, 2048, 2048], P('ep', None, 'tp'), may hold values from -0.125 to 0.125
- down_weight: bfloat16 [8, 2048, 2048], P('ep', 'tp'), may hold values from -0.125 to 0.125
- cotangent: bfloat16 [1024, 2048], P('ep'), may hold values from -0.796875 to 0.796875
Outputs:
- token_grad: bfloat16 [1024, 2048], P('ep')
- router_grad: float32 [2048, 8], P('tp')
- router_rows: float32 [2048], P('tp')
- gate_grad: bfloat16 [8, 2048, 2048], P('ep', None, 'tp')
- up_grad: bfloat16 [8, 2048, 2048], P('ep', None, 'tp')
- down_grad: bfloat16 [8, 2048, 2048], P('ep', 'tp')
- gate_rows: float32 [8, 2048], P('ep')
- up_rows: float32 [8, 2048], P('ep')
- down_rows: float32 [8, 2048], P('ep', 'tp')
Inputs may be any that keep to these rules, and one draw needn't show every extreme that they name: `routing`: A row's 2 experts differ. Within the rows of one index of ep (128 rows), no expert is named more than 56 times, a bound that some block reaches.
All inputs are finite; a program needn't handle non-finite values.
Results may differ from a plain program's by a relative error of at most 0.01.
Values may be sent and summed in bfloat16 or wider, within the bound.
A program may use at most 64 MiB of HBM per device.

v0:
```python
import jax
import jax.numpy as jnp
from jax import lax
from jax.sharding import PartitionSpec as P


def expert_backward(rows_in, cots_in, slot_scale, w_gate, w_up, w_down):
    pre_gate = jnp.dot(rows_in, w_gate, preferred_element_type=jnp.float32)
    pre_up = jnp.dot(rows_in, w_up, preferred_element_type=jnp.float32)
    sigmoid_gate = jax.nn.sigmoid(pre_gate)
    hidden = (pre_gate * sigmoid_gate * pre_up).astype(jnp.bfloat16)
    back_proj = lax.dot_general(
        cots_in, w_down, (((1,), (1,)), ((), ())), preferred_element_type=jnp.float32
    )
    gate_term = jnp.sum(hidden.astype(jnp.float32) * back_proj, axis=1)
    scaled = slot_scale * back_proj
    grad_up_pre = (scaled * pre_gate * sigmoid_gate).astype(jnp.bfloat16)
    grad_gate_pre = (
        scaled * pre_up * sigmoid_gate * (1.0 + pre_gate * (1.0 - sigmoid_gate))
    ).astype(jnp.bfloat16)
    weighted = (slot_scale * cots_in.astype(jnp.float32)).astype(jnp.bfloat16)
    contract_rows = (((0,), (0,)), ((), ()))
    grad_down = lax.dot_general(hidden, weighted, contract_rows, preferred_element_type=jnp.float32)
    grad_gate = lax.dot_general(
        rows_in, grad_gate_pre, contract_rows, preferred_element_type=jnp.float32
    )
    grad_up = lax.dot_general(
        rows_in, grad_up_pre, contract_rows, preferred_element_type=jnp.float32
    )
    contract_hidden = (((1,), (1,)), ((), ()))
    partial_value = lax.dot_general(
        grad_gate_pre, w_gate, contract_hidden, preferred_element_type=jnp.float32
    )
    partial_value = partial_value + lax.dot_general(
        grad_up_pre, w_up, contract_hidden, preferred_element_type=jnp.float32
    )
    return (partial_value, gate_term, grad_gate, grad_up, grad_down)


def per_device(tokens, routing, router_weight, gate_weight, up_weight, down_weight, cotangent):
    groups = lax.axis_size("ep")
    shares = lax.axis_size("tp")
    tok_count, model_width = tokens.shape
    top_count = routing.shape[1]
    local_experts = gate_weight.shape[0]
    experts = local_experts * groups
    capacity = 7 * tok_count * top_count // (4 * experts)
    slot_span = groups * capacity
    assigns = tok_count * top_count
    col_width = model_width // shares
    col_start = lax.axis_index("tp") * col_width
    logits = jnp.dot(tokens, router_weight, preferred_element_type=jnp.float32)
    affinity = jax.nn.sigmoid(logits)
    chosen = jnp.take_along_axis(affinity, routing, axis=1)
    total_aff = jnp.sum(chosen, axis=1, keepdims=True)
    weights = chosen / total_aff
    flat_ids = routing.reshape(-1)
    onehot_ids = (flat_ids[:, None] == jnp.arange(experts, dtype=jnp.int32)[None, :]).astype(
        jnp.int32
    )
    position = jnp.sum((jnp.cumsum(onehot_ids, axis=0) - 1) * onehot_ids, axis=1)
    slot_of = flat_ids % local_experts * slot_span + flat_ids // local_experts * capacity + position
    slot_table = jnp.full((local_experts * slot_span,), assigns, jnp.int32)
    slot_table = slot_table.at[slot_of].set(jnp.arange(assigns, dtype=jnp.int32))
    zero_row = jnp.zeros((1, model_width), jnp.bfloat16)
    tok_pad = jnp.concatenate([tokens, zero_row], axis=0)
    cot_pad = jnp.concatenate([cotangent, zero_row], axis=0)
    weight_pad = jnp.concatenate(
        [weights.astype(jnp.bfloat16).reshape(-1), jnp.zeros((1,), jnp.bfloat16)]
    )
    source_tok = slot_table // top_count
    rows_send = tok_pad[source_tok].reshape(local_experts, groups, capacity, model_width)
    cots_send = cot_pad[source_tok].reshape(local_experts, groups, capacity, model_width)
    scale_send = weight_pad[slot_table].reshape(local_experts, groups, capacity)
    rows_recv, cots_recv, scale_recv = (
        lax.all_to_all(rows_send, "ep", split_axis=1, concat_axis=1, tiled=True),
        lax.all_to_all(cots_send, "ep", split_axis=1, concat_axis=1, tiled=True),
        lax.all_to_all(scale_send, "ep", split_axis=1, concat_axis=1, tiled=True),
    )
    partials, gate_terms, gate_grads, up_grads, down_grads = ([], [], [], [], [])
    slot_scale = scale_recv[0].reshape(slot_span).astype(jnp.float32)[:, None]
    result = expert_backward(
        rows_recv[0].reshape(slot_span, model_width),
        cots_recv[0].reshape(slot_span, model_width),
        slot_scale,
        gate_weight[0],
        up_weight[0],
        down_weight[0],
    )
    partials.append(result[0])
    gate_terms.append(result[1])
    gate_grads.append(result[2])
    up_grads.append(result[3])
    down_grads.append(result[4])
    partial_value = jnp.stack(partials)
    gate_term = jnp.stack(gate_terms)
    grad_gate = jnp.stack(gate_grads)
    grad_up = jnp.stack(up_grads)
    grad_down = jnp.stack(down_grads)
    gate_rows, up_rows = lax.psum(
        (jnp.sum(grad_gate * grad_gate, axis=2), jnp.sum(grad_up * grad_up, axis=2)), "tp"
    )
    down_rows = jnp.sum(grad_down * grad_down, axis=2)
    summed = lax.psum_scatter(partial_value, "tp", scatter_dimension=2, tiled=True)
    gate_sum = lax.psum(gate_term, "tp")
    back_send = summed.astype(jnp.bfloat16).reshape(local_experts, groups, capacity, col_width)
    gate_send = gate_sum.astype(jnp.bfloat16).reshape(local_experts, groups, capacity)
    back_recv, gate_recv = (
        lax.all_to_all(back_send, "ep", split_axis=1, concat_axis=1, tiled=True),
        lax.all_to_all(gate_send, "ep", split_axis=1, concat_axis=1, tiled=True),
    )
    router_cols = lax.dynamic_slice_in_dim(router_weight, col_start, col_width, 0)
    back_flat = back_recv.reshape(local_experts * slot_span, -1)
    back_rows = jnp.sum(
        back_flat[slot_of].astype(jnp.float32).reshape(tok_count, top_count, -1), axis=1
    )
    d_weights = gate_recv.reshape(-1)[slot_of].astype(jnp.float32).reshape(tok_count, top_count)
    d_chosen = (d_weights - jnp.sum(d_weights * weights, axis=1, keepdims=True)) / total_aff
    d_logit = d_chosen * chosen * (1.0 - chosen)
    onehot = (routing[:, :, None] == jnp.arange(experts, dtype=jnp.int32)[None, None, :]).astype(
        jnp.float32
    )
    d_logits = jnp.sum(d_logit[:, :, None] * onehot, axis=1).astype(jnp.bfloat16)
    token_cols = lax.dynamic_slice_in_dim(tokens, col_start, col_width, 1)
    router_part = lax.dot_general(
        token_cols, d_logits, (((0,), (0,)), ((), ())), preferred_element_type=jnp.float32
    )
    router_grad = lax.psum(router_part, "ep")
    router_rows = jnp.sum(router_grad * router_grad, axis=1)
    router_back = lax.dot_general(
        d_logits, router_cols, (((1,), (1,)), ((), ())), preferred_element_type=jnp.float32
    )
    token_grad = (back_rows + router_back).astype(jnp.bfloat16)
    token_grad = lax.all_gather(token_grad, "tp", axis=1, tiled=True)
    return (
        token_grad,
        router_grad,
        router_rows,
        grad_gate.astype(jnp.bfloat16),
        grad_up.astype(jnp.bfloat16),
        grad_down.astype(jnp.bfloat16),
        gate_rows,
        up_rows,
        down_rows,
    )


def solution(mesh):
    return jax.shard_map(
        per_device,
        mesh=mesh,
        in_specs=(
            P("ep", None),
            P("ep", None),
            P(),
            P("ep", None, "tp"),
            P("ep", None, "tp"),
            P("ep", "tp", None),
            P("ep", None),
        ),
        out_specs=(
            P("ep", None),
            P("tp", None),
            P("tp"),
            P("ep", None, "tp"),
            P("ep", None, "tp"),
            P("ep", "tp", None),
            P("ep", None),
            P("ep", None),
            P("ep", "tp"),
        ),
        check_vma=False,
    )
```

profile of v0, /device:TPU:0, one launch (start us, length us, event | category | flops | bytes accessed | tf_op | source)
XLA Modules:
  0.0 255.0 jit_solution(7731860463774829727)
XLA Ops:
  11.0 1.4 scatter_custom_fusion
  12.7 1.3 fusion.14
  14.0 1.4 gather_fusion.5
  16.6 3.2 %gather_fusion = bf16[448]{0:T(512)(128)(2,1)S(1)} fusion(bf16[257]{0:T(512)(128)(2,1)S(1)} %pad_maximum_fusion, s32[1024]{0:T(1024)S(1)} %get-tuple-element.83), kind=kCustom, calls=%fused_computation | custom fusion | bytes 3584 | tf_op jit(solution)/shard_map/gather | solution.py:74
  20.4 7.3 %all-to-all-start = ((bf16[1,8,56]{2,0,1:T(2,128)(2,1)}), bf16[1,8,56]{2,0,1:T(2,128)(2,1)S(1)}, u32[]{:S(2)}, u32[]{:S(2)}) async-start(bf16[1,8,56]{2,0,1:T(2,128)(2,1)} %reshape.229), calls=%async_computation | async-start | bytes 8192 | tf_op jit(solution)/shard_map/all_to_all | solution.py:78
  27.7 3.2 %gather_fusion.2 = bf16[448,2048]{1,0:T(8,128)(2,1)} fusion(bf16[129,2048]{1,0:T(8,128)(2,1)S(1)} %concatenate.11, s32[1024]{0:T(1024)S(1)} %get-tuple-element.82), kind=kCustom, calls=%fused_computation.2 | custom fusion | bytes 3671808 | tf_op jit(solution)/shard_map/gather | solution.py:72
  30.9 3.2 %all-to-all-done = bf16[1,8,56]{2,0,1:T(2,128)(2,1)S(1)} async-done(((bf16[1,8,56]{2,0,1:T(2,128)(2,1)}), bf16[1,8,56]{2,0,1:T(2,128)(2,1)S(1)}, u32[]{:S(2)}, u32[]{:S(2)}) %all-to-all-start) | async-done | bytes 928 | tf_op jit(solution)/shard_map/all_to_all | solution.py:78
  34.1 4.3 %all-to-all-start.2 = ((bf16[1,8,56,2048]{3,2,0,1:T(8,128)(2,1)}), bf16[1,8,56,2048]{3,2,0,1:T(8,128)(2,1)}, u32[]{:S(2)}, u32[]{:S(2)}) async-start(bf16[1,8,56,2048]{3,2,0,1:T(8,128)(2,1)} %bitcast.67), calls=%async_computation.2 | async-start | bytes 3670016 | tf_op jit(solution)/shard_map/all_to_all | solution.py:76
  38.4 1.1 concatenate.10
  39.5 3.2 %gather_fusion.1 = bf16[448,2048]{1,0:T(8,128)(2,1)} fusion(bf16[129,2048]{1,0:T(8,128)(2,1)S(1)} %concatenate.10, s32[1024]{0:T(1024)S(1)} %get-tuple-element.82), kind=kCustom, calls=%fused_computation.1 | custom fusion | bytes 3671808 | tf_op jit(solution)/shard_map/gather | solution.py:73
  42.7 37.2 %all-to-all-done.2 = bf16[1,8,56,2048]{3,2,0,1:T(8,128)(2,1)} async-done(((bf16[1,8,56,2048]{3,2,0,1:T(8,128)(2,1)}), bf16[1,8,56,2048]{3,2,0,1:T(8,128)(2,1)}, u32[]{:S(2)}, u32[]{:S(2)}) %all-to-all-start.2) | async-done | bytes 1835040 | tf_op jit(solution)/shard_map/all_to_all | solution.py:76
  79.9 4.3 %all-to-all-start.1 = ((bf16[1,8,56,2048]{3,2,0,1:T(8,128)(2,1)}), bf16[1,8,56,2048]{3,2,0,1:T(8,128)(2,1)}, u32[]{:S(2)}, u32[]{:S(2)}) async-start(bf16[1,8,56,2048]{3,2,0,1:T(8,128)(2,1)} %bitcast.66), calls=%async_computation.1 | async-start | bytes 3670016 | tf_op jit(solution)/shard_map/all_to_all | solution.py:77
  84.6 4.2 %fusion.5 = f32[448,512]{1,0:T(8,128)} fusion(bf16[448,2048]{1,0:T(8,128)(2,1)} %bitcast.11, bf16[1,2048,512]{2,1,0:T(8,128)(2,1)} %param.11), kind=kOutput, calls=%fused_computation.17 | convolution fusion | flops 939524096 | bytes 4849664 | tf_op jit(solution)/shard_map/dot_general | solution.py:9
  88.8 3.5 %fusion.2 = f32[448,512]{1,0:T(8,128)} fusion(bf16[448,2048]{1,0:T(8,128)(2,1)} %bitcast.11, bf16[1,2048,512]{2,1,0:T(8,128)(2,1)S(1)} %copy-done), kind=kOutput, calls=%fused_computation.14 | convolution fusion | flops 939524096 | bytes 4849664 | tf_op jit(solution)/shard_map/dot_general | solution.py:8
  92.3 34.1 %all-to-all-done.1 = bf16[1,8,56,2048]{3,2,0,1:T(8,128)(2,1)} async-done(((bf16[1,8,56,2048]{3,2,0,1:T(8,128)(2,1)}), bf16[1,8,56,2048]{3,2,0,1:T(8,128)(2,1)}, u32[]{:S(2)}, u32[]{:S(2)}) %all-to-all-start.1) | async-done | bytes 1835040 | tf_op jit(solution)/shard_map/all_to_all | solution.py:77
  126.4 5.5 %multiply_reduce_fusion.3 = (f32[448]{0:T(512)}, bf16[448,512]{1,0:T(8,128)(2,1)}, bf16[448,512]{1,0:T(8,128)(2,1)S(1)}, bf16[448,512]{1,0:T(8,128)(2,1)S(1)}) fusion(f32[448,512]{1,0:T(8,128)} %fusion.5, f32[448,512]{1,0:T(8,128)} %fusion.2, f32[448]{0:T(512)S(1)} %reshape.164, bf16[448,2048]{1,0:T(8,128)(2,1)} %bitcast.7, bf16[1,512,2048]{2,1,0:T(8,128)(2,1)} %param.12), kind=kOutput, calls=%fused_computation.32 | convolution fusion | flops 944111168 | bytes 7147008 | tf_op jit(solution)/shard_map/dot_general | solution.py:12
  131.9 1.1 fusion
  133.5 3.0 %add_bitcast_fusion = f32[1,448,2048]{2,1,0:T(8,128)} fusion(f32[448,2048]{1,0:T(8,128)S(1)} %fusion, bf16[448,512]{1,0:T(8,128)(2,1)S(1)} %get-tuple-element.79, bf16[1,2048,512]{2,1,0:T(8,128)(2,1)S(1)} %copy-done.2), kind=kOutput, calls=%fused_computation.11 | convolution fusion | flops 940441600 | bytes 9895936 | tf_op jit(solution)/shard_map/dot_general | solution.py:34
  136.6 4.1 %convert_bitcast_fusion.2 = (bf16[1,2048,512]{1,2,0:T(8,128)(2,1)}, f32[2048]{0:T(1024)S(1)}) fusion(bf16[448,2048]{1,0:T(8,128)(2,1)} %bitcast.11, bf16[448,512]{1,0:T(8,128)(2,1)S(1)} %get-tuple-element.78), kind=kOutput, calls=%fused_computation.23 | convolution fusion | flops 942667776 | bytes 4399104 | tf_op jit(solution)/shard_map/dot_general | solution.py:24
  140.7 4.3 %convert_bitcast_fusion.1 = (bf16[1,2048,512]{1,2,0:T(8,128)(2,1)}, f32[2048]{0:T(1024)S(1)}) fusion(bf16[448,2048]{1,0:T(8,128)(2,1)} %bitcast.11, bf16[448,512]{1,0:T(8,128)(2,1)S(1)} %get-tuple-element.79), kind=kOutput, calls=%fused_computation.22 | convolution fusion | flops 942667776 | bytes 4399104 | tf_op jit(solution)/shard_map/dot_general | solution.py:27
  145.0 11.0 %all-reduce.2 = (bf16[1,448]{1,0:T(2,128)(2,1)S(1)}, f32[1,2048]{1,0:T(1,128)}, f32[1,2048]{1,0:T(1,128)}) all-reduce(f32[1,448]{1,0:T(1,128)S(1)} %bitcast.73, f32[1,2048]{1,0:T(1,128)S(1)} %bitcast.68, f32[1,2048]{1,0:T(1,128)S(1)} %bitcast.69), channel_id=1, replica_groups=mesh['ep'=8,'tp'=4] {'tp'}, use_global_device_ids=true, to_apply=%region_8.9 | all-reduce | flops 4544 | bytes 35456 | tf_op jit(solution)/shard_map/psum | solution.py:105
  156.7 4.5 %all-to-all-start.4 = ((bf16[1,8,56]{2,0,1:T(2,128)(2,1)}), bf16[1,8,56]{2,0,1:T(2,128)(2,1)S(1)}, u32[]{:S(2)}, u32[]{:S(2)}) async-start(bf16[1,8,56]{2,0,1:T(2,128)(2,1)} %reshape.230), calls=%async_computation.5 | async-start | bytes 8192 | tf_op jit(solution)/shard_map/all_to_all | solution.py:110
  161.3 15.6 %reduce-scatter.2.cloned.1.call-done = f32[1,448,512]{2,1,0:T(8,128)} async-done(((f32[1,448,2048]{2,1,0:T(8,128)}), f32[1,448,512]{2,1,0:T(8,128)}) %reduce-scatter.2.cloned.1.call-update) | async-done | bytes 917520 | tf_op jit(solution)/shard_map/reduce_scatter | solution.py:104
  176.9 2.0 convert_element_type.94
  178.9 5.5 %all-to-all-start.3 = ((bf16[1,8,56,512]{3,2,0,1:T(8,128)(2,1)}), bf16[1,8,56,512]{3,2,0,1:T(8,128)(2,1)S(1)}, u32[]{:S(2)}, u32[]{:S(2)}) async-start(bf16[1,8,56,512]{3,2,0,1:T(8,128)(2,1)} %bitcast.16), calls=%async_computation.4 | async-start | bytes 917504 | tf_op jit(solution)/shard_map/all_to_all | solution.py:109
  184.4 4.9 %multiply_reduce_fusion = (f32[512]{0:T(512)}, bf16[1,512,2048]{2,1,0:T(8,128)(2,1)}) fusion(bf16[448,512]{1,0:T(8,128)(2,1)} %get-tuple-element.67, bf16[448,2048]{1,0:T(8,128)(2,1)} %bitcast.7, f32[448]{0:T(512)S(1)} %copy-done.11), kind=kOutput, calls=%fused_computation.7 | convolution fusion | flops 945421824 | bytes 4394752 | tf_op jit(solution)/shard_map/dot_general | solution.py:23
  189.3 3.9 %copy.90 = bf16[1,2048,512]{2,1,0:T(8,128)(2,1)} copy(bf16[1,2048,512]{1,2,0:T(8,128)(2,1)} %get-tuple-element.76) | data formatting | bytes 4194304
  193.3 3.9 %copy.91 = bf16[1,2048,512]{2,1,0:T(8,128)(2,1)} copy(bf16[1,2048,512]{1,2,0:T(8,128)(2,1)} %get-tuple-element.74) | data formatting | bytes 4194304
  197.3 1.9 gather_fusion.4
  199.7 37.5 %psum.29 = f32[512,8]{0,1:T(8,128)S(1)} all-reduce(f32[512,8]{0,1:T(8,128)S(1)} %fusion.15), channel_id=1, replica_groups=mesh['ep'=8,'tp'=4] {'ep'}, use_global_device_ids=true, to_apply=%region_11.12 | all-reduce | flops 4096 | bytes 32768 | tf_op jit(solution)/shard_map/psum | solution.py:128
  237.8 1.2 gather_fusion.3
  240.9 6.5 %all_gather.3 = bf16[128,2048]{1,0:T(8,128)(2,1)S(1)} all-gather(bf16[128,512]{1,0:T(8,128)(2,1)S(1)} %fusion.11), channel_id=1, replica_groups=mesh['ep'=8,'tp'=4] {'tp'}, dimensions={1}, use_global_device_ids=true | all-gather | bytes 655360 | tf_op jit(solution)/shard_map/all_gather | solution.py:134
  (76 shorter events, 11.2 us)
Async XLA Ops:
  7.2 81.6 %copy-start = (bf16[1,2048,512]{2,1,0:T(8,128)(2,1)S(1)}, bf16[1,2048,512]{2,1,0:T(8,128)(2,1)}, u32[]{:S(2)}) copy-start(bf16[1,2048,512]{2,1,0:T(8,128)(2,1)} %param.10) | copy-start | bytes 6291460
  11.0 1.7 copy-start.7
  14.0 1.6 copy-start.4
  14.0 13.7 %copy-start.1 = (bf16[128,2048]{1,0:T(8,128)(2,1)S(1)}, bf16[128,2048]{1,0:T(8,128)(2,1)}, u32[]{:S(2)}) copy-start(bf16[128,2048]{1,0:T(8,128)(2,1)} %param.7) | copy-start | bytes 1572868
  15.6 15.3 %copy-start.5 = (f32[128]{0:T(128)}, f32[128]{0:T(128)S(1)}, u32[]{:S(2)}) copy-start(f32[128]{0:T(128)S(1)} %get-tuple-element.70) | copy-start | bytes 1540
  20.4 13.7 %all-to-all-start = ((bf16[1,8,56]{2,0,1:T(2,128)(2,1)}), bf16[1,8,56]{2,0,1:T(2,128)(2,1)S(1)}, u32[]{:S(2)}, u32[]{:S(2)}) async-start(bf16[1,8,56]{2,0,1:T(2,128)(2,1)} %reshape.229), calls=%async_computation | async-start | bytes 8192 | tf_op jit(solution)/shard_map/all_to_all | solution.py:78
  34.1 45.8 %all-to-all-start.2 = ((bf16[1,8,56,2048]{3,2,0,1:T(8,128)(2,1)}), bf16[1,8,56,2048]{3,2,0,1:T(8,128)(2,1)}, u32[]{:S(2)}, u32[]{:S(2)}) async-start(bf16[1,8,56,2048]{3,2,0,1:T(8,128)(2,1)} %bitcast.67), calls=%async_computation.2 | async-start | bytes 3670016 | tf_op jit(solution)/shard_map/all_to_all | solution.py:76
  79.9 46.5 %all-to-all-start.1 = ((bf16[1,8,56,2048]{3,2,0,1:T(8,128)(2,1)}), bf16[1,8,56,2048]{3,2,0,1:T(8,128)(2,1)}, u32[]{:S(2)}, u32[]{:S(2)}) async-start(bf16[1,8,56,2048]{3,2,0,1:T(8,128)(2,1)} %bitcast.66), calls=%async_computation.1 | async-start | bytes 3670016 | tf_op jit(solution)/shard_map/all_to_all | solution.py:77
  84.2 92.7 %reduce-scatter.2.cloned.1.call-start = ((), (), s32[]{:S(2)}) async-start(), calls=%async_computation.6 | async-start | bytes 4587520 | tf_op jit(solution)/shard_map/reduce_scatter | solution.py:104
  84.6 41.8 %copy-start.10 = (f32[448]{0:T(512)}, f32[448]{0:T(512)S(1)}, u32[]{:S(2)}) copy-start(f32[448]{0:T(512)S(1)} %reshape.164) | copy-start | bytes 5380
  131.9 1.6 copy-start.2
  140.7 4.3 %copy-start.12 = (f32[448]{0:T(512)S(1)}, f32[448]{0:T(512)}, u32[]{:S(2)}) copy-start(f32[448]{0:T(512)} %get-tuple-element.66) | copy-start | bytes 5380
  140.7 20.6 %copy-start.8 = (s32[256,1]{0,1:T(1,128)S(1)}, s32[256,1]{0,1:T(1,128)}, u32[]{:S(2)}) copy-start(s32[256,1]{0,1:T(1,128)} %copy-done.7) | copy-start | bytes 3076
  145.0 39.4 %copy-start.11 = (f32[448]{0:T(512)S(1)}, f32[448]{0:T(512)}, u32[]{:S(2)}) copy-start(f32[448]{0:T(512)} %copy-done.10) | copy-start | bytes 5380
  156.7 22.2 %all-to-all-start.4 = ((bf16[1,8,56]{2,0,1:T(2,128)(2,1)}), bf16[1,8,56]{2,0,1:T(2,128)(2,1)S(1)}, u32[]{:S(2)}, u32[]{:S(2)}) async-start(bf16[1,8,56]{2,0,1:T(2,128)(2,1)} %reshape.230), calls=%async_computation.5 | async-start | bytes 8192 | tf_op jit(solution)/shard_map/all_to_all | solution.py:110
  178.9 58.9 %all-to-all-start.3 = ((bf16[1,8,56,512]{3,2,0,1:T(8,128)(2,1)}), bf16[1,8,56,512]{3,2,0,1:T(8,128)(2,1)S(1)}, u32[]{:S(2)}, u32[]{:S(2)}) async-start(bf16[1,8,56,512]{3,2,0,1:T(8,128)(2,1)} %bitcast.16), calls=%async_computation.4 | async-start | bytes 917504 | tf_op jit(solution)/shard_map/all_to_all | solution.py:109
  193.3 6.2 %copy-start.9 = (f32[128,2]{0,1:T(2,128)S(1)}, f32[128,2]{0,1:T(2,128)}, u32[]{:S(2)}) copy-start(f32[128,2]{0,1:T(2,128)} %get-tuple-element.69) | copy-start | bytes 3076
  193.3 6.2 %copy-start.6 = (f32[128]{0:T(128)S(1)}, f32[128]{0:T(128)}, u32[]{:S(2)}) copy-start(f32[128]{0:T(128)} %copy-done.5) | copy-start | bytes 1540
  237.2 3.7 %copy-start.3 = (f32[512,8]{0,1:T(8,128)}, f32[512,8]{0,1:T(8,128)S(1)}, u32[]{:S(2)}) copy-start(f32[512,8]{0,1:T(8,128)S(1)} %psum.29) | copy-start | bytes 49156
Sparse Core Ops, SparseCore 0:
  136.7 40.1 reduce-scatter.1
where the time goes:
time: 256 us; the launch traced here: 255 us
  waiting for transfers between devices  90.1 us (35%)
  blocking collectives  55 us (21%)
  matrix products  33.1 us (13%)
  local copies, waits for them, and re-layouts  30 us (12%)
  starting transfers between devices  26.2 us (10%)
  between operations  14.3 us (6%)
  other arithmetic  6.23 us (2%)
    psum x1, blocking collectives, per_device(): router_grad = lax.psum(router_part, 'ep')  37.5 us
    all_to_all x1, waiting for transfers between devices, per_device(): lax.all_to_all(rows_send, 'ep', split_axis=1, concat_axis=1, tiled=True)  37.2 us
    all_to_all x1, waiting for transfers between devices, per_device(): lax.all_to_all(cots_send, 'ep', split_axis=1, concat_axis=1, tiled=True)  34.1 us
    reduce_scatter x1, waiting for transfers between devices, per_device(): lax.psum_scatter(partial_value, 'tp', scatter_dimension=2, tiled=True)  15.6 us
    psum x1, blocking collectives, per_device(): gate_sum = lax.psum(gate_term, 'tp')  11 us
    unnamed x30, local copies, waits for them, and re-layouts  9.92 us
    all_to_all x1, starting transfers between devices, per_device(): lax.all_to_all(scale_send, 'ep', split_axis=1, concat_axis=1, tiled=True)  7.28 us
    all_gather x1, blocking collectives, per_device(): token_grad = lax.all_gather(token_grad, 'tp', axis=1, tiled=True)  6.5 us
  transfers between devices with their start and end apart: 6, of which 4 were waited for; matrix products, arithmetic and copies ran while one was open for 17% of the time, Pallas kernels for 0%

commit v1 on v0

--- a/solution.py
+++ b/solution.py
@@ -2,6 +2,14 @@
 import jax.numpy as jnp
 from jax import lax
 from jax.sharding import PartitionSpec as P
+
+
+def doubling_sum(value, axis):
+    n_dev, total = (lax.axis_size(axis), value)
+    for reach in [1 << k for k in range(n_dev.bit_length() - 1)]:
+        swap = [(i, i ^ reach) for i in range(n_dev)]
+        total = total + lax.ppermute(total, axis, swap)
+    return total
 
 
 def expert_backward(rows_in, cots_in, slot_scale, w_gate, w_up, w_down):
@@ -125,7 +133,7 @@
     router_part = lax.dot_general(
         token_cols, d_logits, (((0,), (0,)), ((), ())), preferred_element_type=jnp.float32
     )
-    router_grad = lax.psum(router_part, "ep")
+    router_grad = doubling_sum(router_part, "ep")
     router_rows = jnp.sum(router_grad * router_grad, axis=1)
     router_back = lax.dot_general(
         d_logits, router_cols, (((1,), (1,)), ((), ())), preferred_element_type=jnp.float32

time: 256 us -> 229 us (0.89)
  blocking collectives: 55 us -> 17.5 us
  waiting for transfers between devices: 90.1 us -> 95.8 us
  starting transfers between devices: 26.2 us -> 30.3 us
    psum x1 -> x0, blocking collectives: 37.5 us -> none  [per_device(): router_grad = lax.psum(router_part, 'ep')]
    reduce_scatter x1, waiting for transfers between devices: 15.6 us -> 6.91 us  [per_device(): lax.psum_scatter(partial_value, 'tp', scatter_dimension=2, tiled=True)]
    ppermute x0 -> x3, waiting for transfers between devices: none -> 8.04 us  [doubling_sum(): total = total + lax.ppermute(total, axis, swap)]
    all_to_all x1, waiting for transfers between devices: 0.01 us -> 6.39 us  [per_device(): lax.all_to_all(gate_send, 'ep', split_axis=1, concat_axis=1, tiled=True)]
    ppermute x0 -> x3, starting transfers between devices: none -> 4.12 us  [doubling_sum(): total = total + lax.ppermute(total, axis, swap)]
    unnamed x30 -> x28, local copies, waits for them, and re-layouts: 9.92 us -> 9.91 us
  transfers between devices with their start and end apart: 6 -> 9, of which waited for: 4 -> 7; matrix products, arithmetic and copies ran while one was open for 17% -> 18% of each run, Pallas kernels for 0% -> 0%
where the time goes in v1:
time: 229 us; the launch traced here: 228 us
  waiting for transfers between devices  95.8 us (42%)
  matrix products  33.1 us (14%)
  starting transfers between devices  30.3 us (13%)
  local copies, waits for them, and re-layouts  30 us (13%)
  blocking collectives  17.5 us (8%)
  between operations  14.3 us (6%)
  other arithmetic  6.74 us (3%)
    all_to_all x1, waiting for transfers between devices, per_device(): lax.all_to_all(rows_send, 'ep', split_axis=1, concat_axis=1, tiled=True)  37.2 us
    all_to_all x1, waiting for transfers between devices, per_device(): lax.all_to_all(cots_send, 'ep', split_axis=1, concat_axis=1, tiled=True)  34.1 us
    psum x1, blocking collectives, per_device(): gate_sum = lax.psum(gate_term, 'tp')  11 us
    unnamed x28, local copies, waits for them, and re-layouts  9.91 us
    ppermute x3, waiting for transfers between devices, doubling_sum(): total = total + lax.ppermute(total, axis, swap)  8.04 us
    all_to_all x1, starting transfers between devices, per_device(): lax.all_to_all(scale_send, 'ep', split_axis=1, concat_axis=1, tiled=True)  7.28 us
    reduce_scatter x1, waiting for transfers between devices, per_device(): lax.psum_scatter(partial_value, 'tp', scatter_dimension=2, tiled=True)  6.91 us
    all_gather x1, blocking collectives, per_device(): token_grad = lax.all_gather(token_grad, 'tp', axis=1, tiled=True)  6.5 us
  transfers between devices with their start and end apart: 9, of which 7 were waited for; matrix products, arithmetic and copies ran while one was open for 18% of the time, Pallas kernels for 0%

profile of v1, /device:TPU:0, one launch (start us, length us, event | category | flops | bytes accessed | tf_op | source)
XLA Modules:
  0.0 227.8 jit_solution(2855601267378167343)
XLA Ops:
  11.0 1.4 scatter_custom_fusion
  14.0 1.4 gather_fusion.5
  16.5 3.2 %gather_fusion = bf16[448]{0:T(512)(128)(2,1)S(1)} fusion(bf16[257]{0:T(512)(128)(2,1)S(1)} %pad_maximum_fusion, s32[1024]{0:T(1024)S(1)} %get-tuple-element.85), kind=kCustom, calls=%fused_computation | custom fusion | bytes 3584 | tf_op jit(solution)/shard_map/gather | solution.py:82
  20.3 7.3 %all-to-all-start = ((bf16[1,8,56]{2,0,1:T(2,128)(2,1)}), bf16[1,8,56]{2,0,1:T(2,128)(2,1)S(1)}, u32[]{:S(2)}, u32[]{:S(2)}) async-start(bf16[1,8,56]{2,0,1:T(2,128)(2,1)} %reshape.229), calls=%async_computation | async-start | bytes 8192 | tf_op jit(solution)/shard_map/all_to_all | solution.py:86
  27.7 3.2 %gather_fusion.2 = bf16[448,2048]{1,0:T(8,128)(2,1)} fusion(bf16[129,2048]{1,0:T(8,128)(2,1)S(1)} %concatenate.11, s32[1024]{0:T(1024)S(1)} %get-tuple-element.84), kind=kCustom, calls=%fused_computation.2 | custom fusion | bytes 3671808 | tf_op jit(solution)/shard_map/gather | solution.py:80
  30.9 3.2 %all-to-all-done = bf16[1,8,56]{2,0,1:T(2,128)(2,1)S(1)} async-done(((bf16[1,8,56]{2,0,1:T(2,128)(2,1)}), bf16[1,8,56]{2,0,1:T(2,128)(2,1)S(1)}, u32[]{:S(2)}, u32[]{:S(2)}) %all-to-all-start) | async-done | bytes 928 | tf_op jit(solution)/shard_map/all_to_all | solution.py:86
  34.0 4.3 %all-to-all-start.2 = ((bf16[1,8,56,2048]{3,2,0,1:T(8,128)(2,1)}), bf16[1,8,56,2048]{3,2,0,1:T(8,128)(2,1)}, u32[]{:S(2)}, u32[]{:S(2)}) async-start(bf16[1,8,56,2048]{3,2,0,1:T(8,128)(2,1)} %bitcast.67), calls=%async_computation.2 | async-start | bytes 3670016 | tf_op jit(solution)/shard_map/all_to_all | solution.py:84
  39.4 3.2 %gather_fusion.1 = bf16[448,2048]{1,0:T(8,128)(2,1)} fusion(bf16[129,2048]{1,0:T(8,128)(2,1)S(1)} %concatenate.10, s32[1024]{0:T(1024)S(1)} %get-tuple-element.84), kind=kCustom, calls=%fused_computation.1 | custom fusion | bytes 3671808 | tf_op jit(solution)/shard_map/gather | solution.py:81
  42.6 37.2 %all-to-all-done.2 = bf16[1,8,56,2048]{3,2,0,1:T(8,128)(2,1)} async-done(((bf16[1,8,56,2048]{3,2,0,1:T(8,128)(2,1)}), bf16[1,8,56,2048]{3,2,0,1:T(8,128)(2,1)}, u32[]{:S(2)}, u32[]{:S(2)}) %all-to-all-start.2) | async-done | bytes 1835040 | tf_op jit(solution)/shard_map/all_to_all | solution.py:84
  79.8 4.3 %all-to-all-start.1 = ((bf16[1,8,56,2048]{3,2,0,1:T(8,128)(2,1)}), bf16[1,8,56,2048]{3,2,0,1:T(8,128)(2,1)}, u32[]{:S(2)}, u32[]{:S(2)}) async-start(bf16[1,8,56,2048]{3,2,0,1:T(8,128)(2,1)} %bitcast.66), calls=%async_computation.1 | async-start | bytes 3670016 | tf_op jit(solution)/shard_map/all_to_all | solution.py:85
  84.5 4.2 %fusion.5 = f32[448,512]{1,0:T(8,128)} fusion(bf16[448,2048]{1,0:T(8,128)(2,1)} %bitcast.11, bf16[1,2048,512]{2,1,0:T(8,128)(2,1)} %param.11), kind=kOutput, calls=%fused_computation.17 | convolution fusion | flops 939524096 | bytes 4849664 | tf_op jit(solution)/shard_map/dot_general | solution.py:17
  88.7 3.5 %fusion.2 = f32[448,512]{1,0:T(8,128)} fusion(bf16[448,2048]{1,0:T(8,128)(2,1)} %bitcast.11, bf16[1,2048,512]{2,1,0:T(8,128)(2,1)S(1)} %copy-done), kind=kOutput, calls=%fused_computation.14 | convolution fusion | flops 939524096 | bytes 4849664 | tf_op jit(solution)/shard_map/dot_general | solution.py:16
  92.2 34.1 %all-to-all-done.1 = bf16[1,8,56,2048]{3,2,0,1:T(8,128)(2,1)} async-done(((bf16[1,8,56,2048]{3,2,0,1:T(8,128)(2,1)}), bf16[1,8,56,2048]{3,2,0,1:T(8,128)(2,1)}, u32[]{:S(2)}, u32[]{:S(2)}) %all-to-all-start.1) | async-done | bytes 1835040 | tf_op jit(solution)/shard_map/all_to_all | solution.py:85
  126.3 5.5 %multiply_reduce_fusion.3 = (f32[448]{0:T(512)}, bf16[448,512]{1,0:T(8,128)(2,1)}, bf16[448,512]{1,0:T(8,128)(2,1)S(1)}, bf16[448,512]{1,0:T(8,128)(2,1)S(1)}) fusion(f32[448,512]{1,0:T(8,128)} %fusion.5, f32[448,512]{1,0:T(8,128)} %fusion.2, f32[448]{0:T(512)S(1)} %reshape.164, bf16[448,2048]{1,0:T(8,128)(2,1)} %bitcast.7, bf16[1,512,2048]{2,1,0:T(8,128)(2,1)} %param.12), kind=kOutput, calls=%fused_computation.32 | convolution fusion | flops 944111168 | bytes 7147008 | tf_op jit(solution)/shard_map/dot_general | solution.py:20
  133.4 3.0 %add_bitcast_fusion = f32[1,448,2048]{2,1,0:T(8,128)} fusion(f32[448,2048]{1,0:T(8,128)S(1)} %fusion, bf16[448,512]{1,0:T(8,128)(2,1)S(1)} %get-tuple-element.81, bf16[1,2048,512]{2,1,0:T(8,128)(2,1)S(1)} %copy-done.2), kind=kOutput, calls=%fused_computation.11 | convolution fusion | flops 940441600 | bytes 9895936 | tf_op jit(solution)/shard_map/dot_general | solution.py:42
  136.5 4.1 %convert_bitcast_fusion.2 = (bf16[1,2048,512]{1,2,0:T(8,128)(2,1)}, f32[2048]{0:T(1024)S(1)}) fusion(bf16[448,2048]{1,0:T(8,128)(2,1)} %bitcast.11, bf16[448,512]{1,0:T(8,128)(2,1)S(1)} %get-tuple-element.80), kind=kOutput, calls=%fused_computation.23 | convolution fusion | flops 942667776 | bytes 4399104 | tf_op jit(solution)/shard_map/dot_general | solution.py:32
  140.6 4.3 %convert_bitcast_fusion.1 = (bf16[1,2048,512]{1,2,0:T(8,128)(2,1)}, f32[2048]{0:T(1024)S(1)}) fusion(bf16[448,2048]{1,0:T(8,128)(2,1)} %bitcast.11, bf16[448,512]{1,0:T(8,128)(2,1)S(1)} %get-tuple-element.81), kind=kOutput, calls=%fused_computation.22 | convolution fusion | flops 942667776 | bytes 4399104 | tf_op jit(solution)/shard_map/dot_general | solution.py:35
  144.9 11.0 %all-reduce.2 = (bf16[1,448]{1,0:T(2,128)(2,1)S(1)}, f32[1,2048]{1,0:T(1,128)}, f32[1,2048]{1,0:T(1,128)}) all-reduce(f32[1,448]{1,0:T(1,128)S(1)} %bitcast.73, f32[1,2048]{1,0:T(1,128)S(1)} %bitcast.68, f32[1,2048]{1,0:T(1,128)S(1)} %bitcast.69), channel_id=1, replica_groups=mesh['ep'=8,'tp'=4] {'tp'}, use_global_device_ids=true, to_apply=%region_8.9 | all-reduce | flops 4544 | bytes 35456 | tf_op jit(solution)/shard_map/psum | solution.py:113
  156.6 4.5 %all-to-all-start.4 = ((bf16[1,8,56]{2,0,1:T(2,128)(2,1)}), bf16[1,8,56]{2,0,1:T(2,128)(2,1)S(1)}, u32[]{:S(2)}, u32[]{:S(2)}) async-start(bf16[1,8,56]{2,0,1:T(2,128)(2,1)} %reshape.230), calls=%async_computation.5 | async-start | bytes 8192 | tf_op jit(solution)/shard_map/all_to_all | solution.py:118
  161.2 6.4 %all-to-all-done.4 = bf16[1,8,56]{2,0,1:T(2,128)(2,1)S(1)} async-done(((bf16[1,8,56]{2,0,1:T(2,128)(2,1)}), bf16[1,8,56]{2,0,1:T(2,128)(2,1)S(1)}, u32[]{:S(2)}, u32[]{:S(2)}) %all-to-all-start.4) | async-done | bytes 928 | tf_op jit(solution)/shard_map/all_to_all | solution.py:118
  167.7 1.9 gather_fusion.4
  169.9 6.9 %reduce-scatter.2.cloned.1.call-done = f32[1,448,512]{2,1,0:T(8,128)} async-done(((f32[1,448,2048]{2,1,0:T(8,128)}), f32[1,448,512]{2,1,0:T(8,128)}) %reduce-scatter.2.cloned.1.call-update) | async-done | bytes 917520 | tf_op jit(solution)/shard_map/reduce_scatter | solution.py:112
  176.8 2.0 convert_element_type.94
  178.8 5.5 %all-to-all-start.3 = ((bf16[1,8,56,512]{3,2,0,1:T(8,128)(2,1)}), bf16[1,8,56,512]{3,2,0,1:T(8,128)(2,1)S(1)}, u32[]{:S(2)}, u32[]{:S(2)}) async-start(bf16[1,8,56,512]{3,2,0,1:T(8,128)(2,1)} %bitcast.16), calls=%async_computation.4 | async-start | bytes 917504 | tf_op jit(solution)/shard_map/all_to_all | solution.py:117
  184.4 2.0 collective-permute-start
  186.5 4.3 %collective-permute-done = f32[512,8]{0,1:T(8,128)S(1)} collective-permute-done((f32[512,8]{0,1:T(8,128)S(1)}, f32[512,8]{0,1:T(8,128)S(1)}, u32[]{:S(2)}, u32[]{:S(2)}) %collective-permute-start) | collective-permute-done | bytes 16416 | tf_op jit(solution)/shard_map/ppermute | solution.py:11
  191.0 3.8 %collective-permute-done.1 = f32[512,8]{0,1:T(8,128)S(1)} collective-permute-done((f32[512,8]{0,1:T(8,128)S(1)}, f32[512,8]{0,1:T(8,128)S(1)}, u32[]{:S(2)}, u32[]{:S(2)}) %collective-permute-start.1) | collective-permute-done | bytes 16416 | tf_op jit(solution)/shard_map/ppermute | solution.py:11
  194.8 1.9 collective-permute-start.2
  196.6 4.9 %multiply_reduce_fusion = (f32[512]{0:T(512)}, bf16[1,512,2048]{2,1,0:T(8,128)(2,1)}) fusion(bf16[448,512]{1,0:T(8,128)(2,1)} %get-tuple-element.69, bf16[448,2048]{1,0:T(8,128)(2,1)} %bitcast.7, f32[448]{0:T(512)S(1)} %copy-done.10), kind=kOutput, calls=%fused_computation.7 | convolution fusion | flops 945421824 | bytes 4394752 | tf_op jit(solution)/shard_map/dot_general | solution.py:31
  201.6 3.9 %copy.90 = bf16[1,2048,512]{2,1,0:T(8,128)(2,1)} copy(bf16[1,2048,512]{1,2,0:T(8,128)(2,1)} %get-tuple-element.78) | data formatting | bytes 4194304
  205.5 3.9 %copy.91 = bf16[1,2048,512]{2,1,0:T(8,128)(2,1)} copy(bf16[1,2048,512]{1,2,0:T(8,128)(2,1)} %get-tuple-element.76) | data formatting | bytes 4194304
  213.6 6.5 %all_gather.3 = bf16[128,2048]{1,0:T(8,128)(2,1)S(1)} all-gather(bf16[128,512]{1,0:T(8,128)(2,1)S(1)} %fusion.11), channel_id=1, replica_groups=mesh['ep'=8,'tp'=4] {'tp'}, dimensions={1}, use_global_device_ids=true | all-gather | bytes 655360 | tf_op jit(solution)/shard_map/all_gather | solution.py:142
  (81 shorter events, 16.6 us)
Async XLA Ops:
  7.2 81.5 %copy-start = (bf16[1,2048,512]{2,1,0:T(8,128)(2,1)S(1)}, bf16[1,2048,512]{2,1,0:T(8,128)(2,1)}, u32[]{:S(2)}) copy-start(bf16[1,2048,512]{2,1,0:T(8,128)(2,1)} %param.10) | copy-start | bytes 6291460
  11.0 1.7 copy-start.6
  14.0 1.6 copy-start.3
  14.0 13.6 %copy-start.1 = (bf16[128,2048]{1,0:T(8,128)(2,1)S(1)}, bf16[128,2048]{1,0:T(8,128)(2,1)}, u32[]{:S(2)}) copy-start(bf16[128,2048]{1,0:T(8,128)(2,1)} %param.7) | copy-start | bytes 1572868
  15.6 15.2 %copy-start.4 = (f32[128]{0:T(128)}, f32[128]{0:T(128)S(1)}, u32[]{:S(2)}) copy-start(f32[128]{0:T(128)S(1)} %get-tuple-element.72) | copy-start | bytes 1540
  20.3 13.7 %all-to-all-start = ((bf16[1,8,56]{2,0,1:T(2,128)(2,1)}), bf16[1,8,56]{2,0,1:T(2,128)(2,1)S(1)}, u32[]{:S(2)}, u32[]{:S(2)}) async-start(bf16[1,8,56]{2,0,1:T(2,128)(2,1)} %reshape.229), calls=%async_computation | async-start | bytes 8192 | tf_op jit(solution)/shard_map/all_to_all | solution.py:86
  34.0 45.8 %all-to-all-start.2 = ((bf16[1,8,56,2048]{3,2,0,1:T(8,128)(2,1)}), bf16[1,8,56,2048]{3,2,0,1:T(8,128)(2,1)}, u32[]{:S(2)}, u32[]{:S(2)}) async-start(bf16[1,8,56,2048]{3,2,0,1:T(8,128)(2,1)} %bitcast.67), calls=%async_computation.2 | async-start | bytes 3670016 | tf_op jit(solution)/shard_map/all_to_all | solution.py:84
  79.8 46.5 %all-to-all-start.1 = ((bf16[1,8,56,2048]{3,2,0,1:T(8,128)(2,1)}), bf16[1,8,56,2048]{3,2,0,1:T(8,128)(2,1)}, u32[]{:S(2)}, u32[]{:S(2)}) async-start(bf16[1,8,56,2048]{3,2,0,1:T(8,128)(2,1)} %bitcast.66), calls=%async_computation.1 | async-start | bytes 3670016 | tf_op jit(solution)/shard_map/all_to_all | solution.py:85
  84.2 92.7 %reduce-scatter.2.cloned.1.call-start = ((), (), s32[]{:S(2)}) async-start(), calls=%async_computation.6 | async-start | bytes 4587520 | tf_op jit(solution)/shard_map/reduce_scatter | solution.py:112
  84.5 41.8 %copy-start.9 = (f32[448]{0:T(512)}, f32[448]{0:T(512)S(1)}, u32[]{:S(2)}) copy-start(f32[448]{0:T(512)S(1)} %reshape.164) | copy-start | bytes 5380
  131.8 1.6 copy-start.2
  140.6 4.3 %copy-start.11 = (f32[448]{0:T(512)S(1)}, f32[448]{0:T(512)}, u32[]{:S(2)}) copy-start(f32[448]{0:T(512)} %get-tuple-element.68) | copy-start | bytes 5380
  140.6 20.6 %copy-start.7 = (s32[256,1]{0,1:T(1,128)S(1)}, s32[256,1]{0,1:T(1,128)}, u32[]{:S(2)}) copy-start(s32[256,1]{0,1:T(1,128)} %copy-done.6) | copy-start | bytes 3076
  140.6 29.2 %copy-start.8 = (f32[128,2]{0,1:T(2,128)S(1)}, f32[128,2]{0,1:T(2,128)}, u32[]{:S(2)}) copy-start(f32[128,2]{0,1:T(2,128)} %get-tuple-element.71) | copy-start | bytes 3076
  140.6 29.3 %copy-start.5 = (f32[128]{0:T(128)S(1)}, f32[128]{0:T(128)}, u32[]{:S(2)}) copy-start(f32[128]{0:T(128)} %copy-done.4) | copy-start | bytes 1540
  144.9 51.7 %copy-start.10 = (f32[448]{0:T(512)S(1)}, f32[448]{0:T(512)}, u32[]{:S(2)}) copy-start(f32[448]{0:T(512)} %copy-done.9) | copy-start | bytes 5380
  156.6 11.0 %all-to-all-start.4 = ((bf16[1,8,56]{2,0,1:T(2,128)(2,1)}), bf16[1,8,56]{2,0,1:T(2,128)(2,1)S(1)}, u32[]{:S(2)}, u32[]{:S(2)}) async-start(bf16[1,8,56]{2,0,1:T(2,128)(2,1)} %reshape.230), calls=%async_computation.5 | async-start | bytes 8192 | tf_op jit(solution)/shard_map/all_to_all | solution.py:118
  178.8 31.7 %all-to-all-start.3 = ((bf16[1,8,56,512]{3,2,0,1:T(8,128)(2,1)}), bf16[1,8,56,512]{3,2,0,1:T(8,128)(2,1)S(1)}, u32[]{:S(2)}, u32[]{:S(2)}) async-start(bf16[1,8,56,512]{3,2,0,1:T(8,128)(2,1)} %bitcast.16), calls=%async_computation.4 | async-start | bytes 917504 | tf_op jit(solution)/shard_map/all_to_all | solution.py:117
  184.4 6.3 %collective-permute-start = (f32[512,8]{0,1:T(8,128)S(1)}, f32[512,8]{0,1:T(8,128)S(1)}, u32[]{:S(2)}, u32[]{:S(2)}) collective-permute-start(f32[512,8]{0,1:T(8,128)S(1)} %fusion.15), channel_id=1, source_target_pairs={{0,4},{4,0},{8,12},{12,8},{16,20},{20,16},{24,28},{28,24},{1,5},{5... | collective-permute-start | bytes 49160 | tf_op jit(solution)/shard_map/ppermute | solution.py:11
  190.7 4.0 %collective-permute-start.1 = (f32[512,8]{0,1:T(8,128)S(1)}, f32[512,8]{0,1:T(8,128)S(1)}, u32[]{:S(2)}, u32[]{:S(2)}) collective-permute-start(f32[512,8]{0,1:T(8,128)S(1)} %add.109), channel_id=1, source_target_pairs={{0,8},{4,12},{8,0},{12,4},{16,24},{20,28},{24,16},{28,20},{1,9},{5... | collective-permute-start | bytes 49160 | tf_op jit(solution)/shard_map/ppermute | solution.py:11
  194.8 14.6 %collective-permute-start.2 = (f32[512,8]{0,1:T(8,128)S(1)}, f32[512,8]{0,1:T(8,128)S(1)}, u32[]{:S(2)}, u32[]{:S(2)}) collective-permute-start(f32[512,8]{0,1:T(8,128)S(1)} %add.110), channel_id=1, source_target_pairs={{0,16},{4,20},{8,24},{12,28},{16,0},{20,4},{24,8},{28,12},{1,17},{... | collective-permute-start | bytes 49160 | tf_op jit(solution)/shard_map/ppermute | solution.py:11
Sparse Core Ops, SparseCore 0:
  136.6 40.1 reduce-scatter.1
